TPU v7x, 32 devices: a whole 2x2x4 slice. The times are simulated.
32 devices in a mesh: sp: 16 (over z, y, x), dp: 2 (over core).
Axes of the slice: x: 2, y: 2, z: 4, core: 2. Of those that a mesh axis runs over, the one named last changes fastest.
Arguments:
- inputs: bfloat16 [2, 2048, 2048], P('dp', 'sp'), may hold values from -6 to 6
- conv_weight: bfloat16 [4, 2048], replicated, may hold values from -3 to 3
- gate_weight: bfloat16 [2, 8, 256, 256], P(None, 'dp'), may hold values from -0.375 to 0.375
- rate_param: float32 [2048], replicated, may hold values from 4 to 12.5
- pace: float32 [2, 2048], P('dp'), may hold values from 0.5 to 30000
Outputs:
- recurrent: bfloat16 [2, 2048, 2048], P('dp', 'sp')
All inputs are finite; a program needn't handle non-finite values.
Results may differ from a plain program's by a relative error of at most 0.008.
Values may be sent and summed in bfloat16 or wider, within the bound.
A program may use at most 128 MiB of HBM per device.

v0:
```python
import jax
import jax.numpy as jnp
from jax import lax
from jax.sharding import PartitionSpec as P

HEADS = 8
BLOCK = 256
CONV = 4
gate_power = 8.0


def passed_along(array, axis, by):
    devices = lax.axis_size(axis)
    pairs = [(i, i + by) for i in range(devices) if 0 <= i + by < devices]
    return lax.ppermute(array, axis, pairs)


def combine(earlier, later):
    decay_e, state_e = earlier
    decay_l, state_l = later
    return (decay_e * decay_l, decay_l * state_e + state_l)


def lru_terms(pre_recur, pre_input, values, rate_col, pace_col):
    recur_gate = jax.nn.sigmoid(pre_recur.astype(jnp.float32))
    input_gate = jax.nn.sigmoid(pre_input.astype(jnp.float32))
    log_decay = -gate_power * pace_col * recur_gate * jax.nn.softplus(-rate_col)
    decay = jnp.exp(log_decay)
    drive = jnp.sqrt(-jnp.expm1(2.0 * log_decay)) * input_gate * values.astype(jnp.float32)
    return (decay, drive)


def body(inputs, conv_weight, gate_weight, rate_param, pace):
    own_rows = inputs[0].T
    width = own_rows.shape[0]
    count = own_rows.shape[1]
    earlier = passed_along(own_rows[:, count - (CONV - 1) :], "sp", 1)
    padded = jnp.concatenate([earlier, own_rows], axis=1).astype(jnp.float32)
    conv_taps = conv_weight.astype(jnp.float32)
    conv_out = jnp.zeros((width, count), jnp.float32)
    for tap in range(CONV):
        conv_out = conv_out + conv_taps[tap][:, None] * padded[:, tap : tap + count]
    conv_out = conv_out.astype(jnp.bfloat16)
    by_head = conv_out.reshape(HEADS, BLOCK, count)
    preact = (
        jnp.einsum(
            "hit,ghij->ghjt",
            by_head,
            lax.all_gather(gate_weight, "dp", axis=1, tiled=True),
            preferred_element_type=jnp.float32,
        )
        .astype(jnp.bfloat16)
        .reshape(2, width, count)
    )
    stacked = jnp.stack([conv_out, preact[0], preact[1]])
    arrived = lax.all_to_all(stacked, "sp", split_axis=1, concat_axis=2, tiled=True)
    lanes = arrived.shape[1]
    lane_rates = lax.dynamic_slice_in_dim(rate_param, lax.axis_index("sp") * lanes, lanes)
    decay, drive = lru_terms(
        arrived[1], arrived[2], arrived[0], lane_rates[:, None], pace[0][None, :]
    )
    _, state = lax.associative_scan(combine, (decay, drive), axis=1)
    result = lax.all_to_all(
        state.astype(jnp.bfloat16), "sp", split_axis=1, concat_axis=0, tiled=True
    )
    return result.T[None]


def solution(mesh):
    return jax.shard_map(
        body,
        mesh=mesh,
        in_specs=(P("dp", "sp", None), P(), P(None, "dp", None, None), P(), P("dp", None)),
        out_specs=P("dp", "sp", None),
        check_vma=False,
    )
```

profile of v0, /device:TPU:0, one launch (start us, length us, event | category | flops | bytes accessed | tf_op | source)
XLA Modules:
  0.0 151.2 jit_solution(12866272480589293699)
XLA Ops:
  6.5 0.0 all-gather.2.cloned.1.call-start
  6.5 2.3 %copy.31 = bf16[2,4,256,256]{3,2,0,1:T(8,128)(2,1)} copy(bf16[2,4,256,256]{3,2,1,0:T(8,128)(2,1)} %param.7) | data formatting | bytes 2097152 | tf_op args[2]
  8.9 0.0 all-gather.2.cloned.1.call-update
  8.9 0.0 copy-done.2
  8.9 0.3 copy.30
  9.2 0.2 slice.406
  9.4 4.9 %collective-permute-start = (bf16[2048,3]{1,0:T(8,128)(2,1)S(1)}, bf16[2048,3]{1,0:T(8,128)(2,1)S(1)}, u32[]{:S(2)}, u32[]{:S(2)}) collective-permute-start(bf16[2048,3]{1,0:T(8,128)(2,1)S(1)} %slice.406), channel_id=1, source_target_pairs={{0,2},{2,4},{4,6},{6,8},{8,10},{10,12},{12,14},{14,16},{16,18},{18... | collective-permute-start | bytes 36872 | tf_op jit(solution)/shard_map/ppermute | solution.py:15
  14.3 0.0 copy-done.3
  14.4 11.1 %collective-permute-done = bf16[2048,3]{1,0:T(8,128)(2,1)S(1)} collective-permute-done((bf16[2048,3]{1,0:T(8,128)(2,1)S(1)}, bf16[2048,3]{1,0:T(8,128)(2,1)S(1)}, u32[]{:S(2)}, u32[]{:S(2)}) %collective-permute-start) | collective-permute-done | bytes 12320 | tf_op jit(solution)/shard_map/ppermute | solution.py:15
  25.4 0.4 maximum_convert_fusion
  25.9 2.2 %fusion.29 = bf16[1,2048,128]{2,1,0:T(8,128)(2,1)S(1)} fusion(f32[2048,131]{1,0:T(8,128)S(1)} %maximum_convert_fusion, f32[2048]{0:T(1024)S(1)} %bitcast.61, f32[2048]{0:T(1024)S(1)} %bitcast.59, f32[2048]{0:T(1024)S(1)} %bitcast.57, f32[2048]{0:T(1024)S(1)} %bitcast.55), kind=kLoop, calls=%fused_computation.75 | loop fusion | flops 2097152 | bytes 4751360 | tf_op jit(solution)/shard_map/stack | solution.py:55
  28.0 2.2 %fusion.2 = bf16[2048,128]{1,0:T(8,128)(2,1)S(1)} fusion(f32[2048,131]{1,0:T(8,128)S(1)} %maximum_convert_fusion, f32[2048]{0:T(1024)S(1)} %bitcast.62, f32[2048]{0:T(1024)S(1)} %bitcast.60, f32[2048]{0:T(1024)S(1)} %bitcast.58, f32[2048]{0:T(1024)S(1)} %bitcast.56), kind=kLoop, calls=%fused_computation.5 | loop fusion | flops 2097152 | bytes 4751360 | tf_op jit(solution)/shard_map/convert_element_type | solution.py:43
  30.2 0.0 all-gather.2.cloned.1.call-done
  30.2 2.1 %fusion = bf16[2,8,256,128]{2,3,0,1:T(8,128)(2,1)S(1)} fusion(bf16[8,256,128,1]{2,1,3,0:T(8,128)(2,1)S(1)} %bitcast.49, bf16[2,8,256,256]{3,2,0,1:T(8,128)(2,1)} %all-gather.2.cloned.1.call-done), kind=kOutput, calls=%fused_computation.2 | convolution fusion | flops 268959744 | bytes 3670016 | tf_op jit(solution)/shard_map/hit,ghij->ghjt/dot_general | solution.py:46
  32.3 0.1 fusion.14
  32.4 0.3 copy.33
  32.7 0.3 copy.34
  33.0 0.2 pad_maximum_fusion
  33.1 10.7 %copy.35 = bf16[3,2048,128]{2,0,1:T(4,128)(2,1)} copy(bf16[3,2048,128]{2,1,0:T(8,128)(2,1)S(1)} %pad_maximum_fusion) | data formatting | bytes 3145728 | tf_op jit(solution)/shard_map/stack | solution.py:55
  43.9 8.0 %all-to-all-start = ((bf16[3,2048,128]{2,0,1:T(4,128)(2,1)}), bf16[3,2048,128]{2,0,1:T(4,128)(2,1)S(1)}, u32[]{:S(2)}, u32[]{:S(2)}) async-start(bf16[3,2048,128]{2,0,1:T(4,128)(2,1)} %copy.35), calls=%async_computation | async-start | bytes 4194304 | tf_op jit(solution)/shard_map/all_to_all | solution.py:56
  51.9 0.8 compare_select_fusion
  52.6 0.0 copy-done.4
  52.7 41.6 %all-to-all-done = bf16[3,2048,128]{2,0,1:T(4,128)(2,1)S(1)} async-done(((bf16[3,2048,128]{2,0,1:T(4,128)(2,1)}), bf16[3,2048,128]{2,0,1:T(4,128)(2,1)S(1)}, u32[]{:S(2)}, u32[]{:S(2)}) %all-to-all-start) | async-done | bytes 1572896 | tf_op jit(solution)/shard_map/all_to_all | solution.py:56
  94.3 0.2 copy.36
  94.5 0.1 slice_convert_fusion
  94.6 0.6 add_divide_fusion.1
  95.2 1.3 copy.39
  96.5 1.4 copy.37
  97.8 1.3 copy.38
  99.2 0.0 copy-done
  99.2 2.4 %fusion.6 = (f32[128,2048]{0,1:T(8,128)S(1)}, f32[128,2048]{0,1:T(8,128)S(1)}) fusion(f32[1,128,16,128]{1,3,2,0:T(8,128)} %copy.37, f32[128]{0:T(128)S(1)} %compare_select_fusion, f32[2048]{0:T(1024)S(1)} %bitcast.63, f32[1,128,16,128]{1,3,2,0:T(8,128)S(1)} %copy-done, f32[1,128,16,128]{1,3,2,0:T(8,128)} %copy.38), kind=kLoop, calls=%fused_computation.19 | loop fusion | flops 1572864 | bytes 5251584 | tf_op jit(solution)/shard_map/exp | solution.py:28
  101.6 0.7 slice.328
  102.3 2.1 %slice.324 = f32[128,1024]{0,1:T(8,128)} slice(f32[128,2048]{0,1:T(8,128)S(1)} %get-tuple-element.7), slice={[0:128:1], [1:2048:2]} | slice | bytes 1048576 | tf_op jit(solution)/shard_map/slice | solution.py:62
  104.4 0.7 slice.323
  105.1 0.0 copy-start.1
  105.1 0.7 slice.404
  105.8 2.0 %slice.326 = f32[128,1024]{0,1:T(8,128)} slice(f32[128,2048]{0,1:T(8,128)S(1)} %get-tuple-element.8), slice={[0:128:1], [1:2048:2]} | slice | bytes 1048576 | tf_op jit(solution)/shard_map/slice | solution.py:62
  107.8 2.0 %slice.325 = f32[128,1024]{0,1:T(8,128)} slice(f32[128,2048]{0,1:T(8,128)S(1)} %get-tuple-element.8), slice={[0:128:1], [0:2047:2]} | slice | bytes 1048576 | tf_op jit(solution)/shard_map/slice | solution.py:62
  109.9 0.0 copy-done.1
  109.9 1.3 fusion.15
  111.2 0.4 slice.334
  111.6 0.4 slice.330
  112.0 0.4 slice.329
  112.4 0.4 slice.402
  112.8 0.4 slice.332
  113.2 1.4 slice.331
  114.6 1.0 fusion.16
  115.6 0.1 slice.340
  115.7 0.1 slice.336
  115.8 0.3 slice.335
  116.1 0.3 slice.400
  116.4 0.1 slice.338
  116.5 0.1 slice.337
  118.2 0.1 fusion.8
  118.3 0.1 pad.85
  118.4 0.1 pad.86
  118.5 0.1 add.207
  118.5 0.1 fusion.7
  118.7 0.1 pad.87
  118.8 0.1 pad.88
  118.9 0.1 add_convert_fusion
  119.0 24.0 %all_to_all.34 = bf16[128,16,128]{0,2,1:T(8,128)(2,1)S(1)} all-to-all(bf16[128,16,128]{0,2,1:T(8,128)(2,1)S(1)} %bitcast.50), channel_id=1, replica_groups=mesh['sp'=16,'dp'=2] {'sp'}, dimensions={1} | all-to-all | bytes 1048576 | tf_op jit(solution)/shard_map/all_to_all | solution.py:63
  143.1 0.3 copy.40
  143.3 1.0 copy.41
  (107 shorter events, 1.3 us)
Async XLA Ops:
  6.5 2.4 %copy-start.2 = (bf16[1,128,2048]{2,1,0:T(8,128)(2,1)S(1)}, bf16[1,128,2048]{2,1,0:T(8,128)(2,1)}, u32[]{:S(2)}) copy-start(bf16[1,128,2048]{2,1,0:T(8,128)(2,1)} %param.5) | copy-start | bytes 1572868
  6.5 23.7 %all-gather.2.cloned.1.call-start = ((), (), s32[]{:S(2)}) async-start(), calls=%async_computation.2 | async-start | bytes 3145728 | tf_op jit(solution)/shard_map/all_gather | solution.py:49
  8.9 5.4 %copy-start.3 = (bf16[4,2048]{1,0:T(4,128)(2,1)S(1)}, bf16[4,2048]{1,0:T(4,128)(2,1)}, u32[]{:S(2)}) copy-start(bf16[4,2048]{1,0:T(4,128)(2,1)} %param.6) | copy-start | bytes 49156
  9.4 16.0 %collective-permute-start = (bf16[2048,3]{1,0:T(8,128)(2,1)S(1)}, bf16[2048,3]{1,0:T(8,128)(2,1)S(1)}, u32[]{:S(2)}, u32[]{:S(2)}) collective-permute-start(bf16[2048,3]{1,0:T(8,128)(2,1)S(1)} %slice.406), channel_id=1, source_target_pairs={{0,2},{2,4},{4,6},{6,8},{8,10},{10,12},{12,14},{14,16},{16,18},{18... | collective-permute-start | bytes 36872 | tf_op jit(solution)/shard_map/ppermute | solution.py:15
  43.9 8.8 %copy-start.4 = (f32[1,2048]{1,0:T(1,128)S(1)}, f32[1,2048]{1,0:T(1,128)}, u32[]{:S(2)}) copy-start(f32[1,2048]{1,0:T(1,128)} %param.9) | copy-start | bytes 24580
  43.9 50.4 %all-to-all-start = ((bf16[3,2048,128]{2,0,1:T(4,128)(2,1)}), bf16[3,2048,128]{2,0,1:T(4,128)(2,1)S(1)}, u32[]{:S(2)}, u32[]{:S(2)}) async-start(bf16[3,2048,128]{2,0,1:T(4,128)(2,1)} %copy.35), calls=%async_computation | async-start | bytes 4194304 | tf_op jit(solution)/shard_map/all_to_all | solution.py:56
  96.5 2.7 %copy-start = (f32[1,128,16,128]{1,3,2,0:T(8,128)S(1)}, f32[1,128,16,128]{1,3,2,0:T(8,128)}, u32[]{:S(2)}) copy-start(f32[1,128,16,128]{1,3,2,0:T(8,128)} %copy.39) | copy-start | bytes 3145732
  105.1 4.8 %copy-start.1 = (f32[128,1024]{0,1:T(8,128)S(1)}, f32[128,1024]{0,1:T(8,128)}, u32[]{:S(2)}) copy-start(f32[128,1024]{0,1:T(8,128)} %slice.324) | copy-start | bytes 1572868
Sparse Core Ops, SparseCore 0:
  9.0 13.2 all-gather.1
where the time goes:
time: 152 us; the launch traced here: 151 us
  waiting for transfers between devices  52.7 us (35%)
  local copies, waits for them, and re-layouts  33.3 us (22%)
  blocking collectives  24 us (16%)
  between operations  14.2 us (9%)
  starting transfers between devices  12.9 us (8%)
  other arithmetic  11.8 us (8%)
  matrix products  2.09 us (1%)
    all_to_all x1, waiting for transfers between devices, body(): lax.all_to_all(stacked, 'sp', split_axis=1, concat_axis=2, tiled=True)  41.6 us
    all_to_all x1, blocking collectives, body(): lax.all_to_all(state.astype(jnp.bfloat16), 'sp', split_axis=1, concat_axi...  24 us
    slice x67, local copies, waits for them, and re-layouts, body(): _, state = lax.associative_scan(combine, (decay, drive), axis=1)  13.2 us
    ppermute x1, waiting for transfers between devices, passed_along(): return lax.ppermute(array, axis, pairs)  11.1 us
    another operation x1, local copies, waits for them, and re-layouts, body(): stacked = jnp.stack([conv_out, preact[0], preact[1]])  10.7 us
    all_to_all x1, starting transfers between devices, body(): lax.all_to_all(stacked, 'sp', split_axis=1, concat_axis=2, tiled=True)  8 us
    ppermute x1, starting transfers between devices, passed_along(): return lax.ppermute(array, axis, pairs)  4.9 us
  transfers between devices with their start and end apart: 3, of which 2 were waited for; matrix products, arithmetic and copies ran while one was open for 4% of the time, Pallas kernels for 0%

commit v1 on v0

--- a/solution.py
+++ b/solution.py
@@ -53,7 +53,12 @@
         .reshape(2, width, count)
     )
     stacked = jnp.stack([conv_out, preact[0], preact[1]])
-    arrived = lax.all_to_all(stacked, "sp", split_axis=1, concat_axis=2, tiled=True)
+    arrived = jnp.concatenate(
+        lax.all_to_all(
+            jnp.stack(jnp.split(stacked, lax.axis_size("sp"), axis=1), axis=0), "sp", 0, 0
+        ),
+        axis=2,
+    )
     lanes = arrived.shape[1]
     lane_rates = lax.dynamic_slice_in_dim(rate_param, lax.axis_index("sp") * lanes, lanes)
     decay, drive = lru_terms(

time: 152 us -> 143 us (0.941)
  waiting for transfers between devices: 52.7 us -> 43.8 us
  blocking collectives: 24 us -> 21.6 us
  other arithmetic: 11.8 us -> 14.1 us
    another operation x1, local copies, waits for them, and re-layouts: 10.7 us -> 0.65 us  [body(): jnp.stack(jnp.split(stacked, lax.axis_size('sp'), axis=1), axis=0)]
    unnamed x12 -> x27, local copies, waits for them, and re-layouts: 2.62 us -> 12.3 us
    all_to_all x1, waiting for transfers between devices: 41.6 us -> 32.7 us  [body(): lax.all_to_all(jnp.stack(jnp.split(stacked, lax.axis_size('sp'), axis=1),...]
    all_to_all x1, blocking collectives: 24 us -> 21.6 us  [body(): lax.all_to_all(state.astype(jnp.bfloat16), 'sp', split_axis=1, concat_axi...]
where the time goes in v1:
time: 143 us
  waiting for transfers between devices  43.8 us (31%)
  local copies, waits for them, and re-layouts  34 us (24%)
  blocking collectives  21.6 us (15%)
  between operations  14.2 us (10%)
  other arithmetic  14.1 us (10%)
  starting transfers between devices  12.9 us (9%)
  matrix products  2.09 us (1%)
    all_to_all x1, waiting for transfers between devices, body(): lax.all_to_all(jnp.stack(jnp.split(stacked, lax.axis_size('sp'), axis=1),...  32.7 us
    all_to_all x1, blocking collectives, body(): lax.all_to_all(state.astype(jnp.bfloat16), 'sp', split_axis=1, concat_axi...  21.6 us
    slice x67, local copies, waits for them, and re-layouts, body(): _, state = lax.associative_scan(combine, (decay, drive), axis=1)  13.2 us
    unnamed x27, local copies, waits for them, and re-layouts  12.3 us
    ppermute x1, waiting for transfers between devices, passed_along(): return lax.ppermute(array, axis, pairs)  11.1 us
    all_to_all x1, starting transfers between devices, body(): lax.all_to_all(jnp.stack(jnp.split(stacked, lax.axis_size('sp'), axis=1),...  7.98 us
    ppermute x1, starting transfers between devices, passed_along(): return lax.ppermute(array, axis, pairs)  4.9 us
  transfers between devices with their start and end apart: 3, of which 2 were waited for; matrix products, arithmetic and copies ran while one was open for 4% of the time, Pallas kernels for 0%

profile of v1, /device:TPU:0, one launch (start us, length us, event | category | flops | bytes accessed | tf_op | source)
XLA Modules:
  0.0 142.7 jit_solution(10216234845656799369)
XLA Ops:
  6.5 2.3 %copy.24 = bf16[2,4,256,256]{3,2,0,1:T(8,128)(2,1)} copy(bf16[2,4,256,256]{3,2,1,0:T(8,128)(2,1)} %param.7) | data formatting | bytes 2097152 | tf_op args[2]
  8.9 0.3 copy.23
  9.2 0.2 slice.406
  9.4 4.9 %collective-permute-start = (bf16[2048,3]{1,0:T(8,128)(2,1)S(1)}, bf16[2048,3]{1,0:T(8,128)(2,1)S(1)}, u32[]{:S(2)}, u32[]{:S(2)}) collective-permute-start(bf16[2048,3]{1,0:T(8,128)(2,1)S(1)} %slice.406), channel_id=1, source_target_pairs={{0,2},{2,4},{4,6},{6,8},{8,10},{10,12},{12,14},{14,16},{16,18},{18... | collective-permute-start | bytes 36872 | tf_op jit(solution)/shard_map/ppermute | solution.py:15
  14.4 11.1 %collective-permute-done = bf16[2048,3]{1,0:T(8,128)(2,1)S(1)} collective-permute-done((bf16[2048,3]{1,0:T(8,128)(2,1)S(1)}, bf16[2048,3]{1,0:T(8,128)(2,1)S(1)}, u32[]{:S(2)}, u32[]{:S(2)}) %collective-permute-start) | collective-permute-done | bytes 12320 | tf_op jit(solution)/shard_map/ppermute | solution.py:15
  25.4 0.4 maximum_convert_fusion
  25.9 2.2 %fusion.45 = bf16[1,2048,128]{2,1,0:T(8,128)(2,1)S(1)} fusion(f32[2048,131]{1,0:T(8,128)S(1)} %maximum_convert_fusion, f32[2048]{0:T(1024)S(1)} %bitcast.123, f32[2048]{0:T(1024)S(1)} %bitcast.121, f32[2048]{0:T(1024)S(1)} %bitcast.119, f32[2048]{0:T(1024)S(1)} %bitcast.117), kind=kLoop, calls=%fused_computation.107 | loop fusion | flops 2097152 | bytes 4751360 | tf_op jit(solution)/shard_map/stack | solution.py:55
  28.0 2.2 %fusion.2 = bf16[2048,128]{1,0:T(8,128)(2,1)S(1)} fusion(f32[2048,131]{1,0:T(8,128)S(1)} %maximum_convert_fusion, f32[2048]{0:T(1024)S(1)} %bitcast.124, f32[2048]{0:T(1024)S(1)} %bitcast.122, f32[2048]{0:T(1024)S(1)} %bitcast.120, f32[2048]{0:T(1024)S(1)} %bitcast.118), kind=kLoop, calls=%fused_computation.5 | loop fusion | flops 2097152 | bytes 4751360 | tf_op jit(solution)/shard_map/convert_element_type | solution.py:43
  30.2 2.1 %fusion = bf16[2,8,256,128]{2,3,0,1:T(8,128)(2,1)S(1)} fusion(bf16[8,256,128,1]{2,1,3,0:T(8,128)(2,1)S(1)} %bitcast.111, bf16[2,8,256,256]{3,2,0,1:T(8,128)(2,1)} %all-gather.2.cloned.1.call-done), kind=kOutput, calls=%fused_computation.2 | convolution fusion | flops 268959744 | bytes 3670016 | tf_op jit(solution)/shard_map/hit,ghij->ghjt/dot_general | solution.py:46
  32.4 0.3 copy.26
  32.7 0.3 copy.27
  33.0 0.2 pad_maximum_fusion
  33.1 0.6 fusion.25
  33.8 0.6 fusion.24
  34.4 0.6 fusion.23
  35.1 0.6 fusion.22
  35.7 0.7 fusion.21
  36.4 0.7 fusion.20
  37.0 0.7 fusion.19
  37.7 0.6 fusion.18
  38.3 0.7 fusion.17
  39.0 0.7 fusion.16
  39.6 0.6 fusion.15
  40.3 0.6 fusion.14
  40.9 0.6 fusion.13
  41.5 0.7 fusion.12
  42.2 0.6 fusion.11
  42.8 0.6 fusion.10
  43.5 8.0 %all-to-all-start = ((bf16[16,3,128,128]{3,2,1,0:T(8,128)(2,1)}), bf16[16,3,128,128]{3,2,1,0:T(8,128)(2,1)S(1)}, u32[]{:S(2)}, u32[]{:S(2)}) async-start(bf16[16,3,128,128]{3,2,1,0:T(8,128)(2,1)} %fusion.10), calls=%async_computation | async-start | bytes 3145728 | tf_op jit(solution)/shard_map/all_to_all | solution.py:57
  51.5 0.8 compare_select_fusion
  52.3 32.7 %all-to-all-done = bf16[16,3,128,128]{3,2,1,0:T(8,128)(2,1)S(1)} async-done(((bf16[16,3,128,128]{3,2,1,0:T(8,128)(2,1)}), bf16[16,3,128,128]{3,2,1,0:T(8,128)(2,1)S(1)}, u32[]{:S(2)}, u32[]{:S(2)}) %all-to-all-start) | async-done | bytes 1572896 | tf_op jit(solution)/shard_map/all_to_all | solution.py:57
  85.0 1.1 slice_convert_fusion
  86.0 1.5 %add_divide_fusion.1 = (f32[1,128,16,128]{3,1,0,2:T(8,128)}, f32[1,128,16,128]{3,1,0,2:T(8,128)S(1)}) fusion(bf16[3,128,16,128]{3,1,0,2:T(8,128)(2,1)S(1)} %bitcast.108), kind=kLoop, calls=%fused_computation.18 | loop fusion | flops 2097152 | bytes 3145728 | tf_op jit(solution)/shard_map/div | solution.py:25
  87.6 2.7 %copy.30 = f32[1,128,16,128]{1,3,2,0:T(8,128)} copy(f32[1,128,16,128]{3,1,0,2:T(8,128)} %slice_convert_fusion) | data formatting | bytes 2097152 | tf_op jit(solution)/shard_map/convert_element_type | solution.py:29
  90.2 1.3 copy.28
  91.5 1.3 copy.29
  92.8 2.7 %fusion.6 = (f32[128,2048]{0,1:T(8,128)S(1)}, f32[128,2048]{0,1:T(8,128)S(1)}) fusion(f32[1,128,16,128]{1,3,2,0:T(8,128)} %copy.28, f32[128]{0:T(128)S(1)} %compare_select_fusion, f32[2048]{0:T(1024)S(1)} %bitcast.125, f32[1,128,16,128]{1,3,2,0:T(8,128)} %copy.30, f32[1,128,16,128]{1,3,2,0:T(8,128)} %copy.29), kind=kLoop, calls=%fused_computation.19 | loop fusion | flops 1572864 | bytes 5251584 | tf_op jit(solution)/shard_map/exp | solution.py:28
  95.6 0.7 slice.328
  96.3 2.1 %slice.324 = f32[128,1024]{0,1:T(8,128)} slice(f32[128,2048]{0,1:T(8,128)S(1)} %get-tuple-element.7), slice={[0:128:1], [1:2048:2]} | slice | bytes 1048576 | tf_op jit(solution)/shard_map/slice | solution.py:67
  98.3 0.7 slice.323
  99.0 0.7 slice.404
  99.8 2.0 %slice.326 = f32[128,1024]{0,1:T(8,128)} slice(f32[128,2048]{0,1:T(8,128)S(1)} %get-tuple-element.8), slice={[0:128:1], [1:2048:2]} | slice | bytes 1048576 | tf_op jit(solution)/shard_map/slice | solution.py:67
  101.8 2.0 %slice.325 = f32[128,1024]{0,1:T(8,128)} slice(f32[128,2048]{0,1:T(8,128)S(1)} %get-tuple-element.8), slice={[0:128:1], [0:2047:2]} | slice | bytes 1048576 | tf_op jit(solution)/shard_map/slice | solution.py:67
  103.9 1.3 fusion.31
  105.2 0.4 slice.334
  105.6 0.4 slice.330
  106.0 0.4 slice.329
  106.4 0.4 slice.402
  106.8 0.4 slice.332
  107.2 1.4 slice.331
  108.6 1.0 fusion.32
  109.6 0.1 slice.340
  109.7 0.1 slice.336
  109.8 0.3 slice.335
  110.1 0.3 slice.400
  110.4 0.1 slice.338
  110.5 0.1 slice.337
  112.5 0.1 fusion.7
  112.6 0.1 pad.87
  112.8 0.1 pad.88
  112.9 0.1 add_convert_fusion
  113.0 21.6 %all_to_all.24 = bf16[128,16,128]{0,2,1:T(8,128)(2,1)S(1)} all-to-all(bf16[128,16,128]{0,2,1:T(8,128)(2,1)S(1)} %bitcast.112), channel_id=1, replica_groups=mesh['sp'=16,'dp'=2] {'sp'}, dimensions={1} | all-to-all | bytes 1048576 | tf_op jit(solution)/shard_map/all_to_all | solution.py:68
  134.6 0.3 copy.31
  134.9 1.0 copy.32
  (121 shorter events, 1.6 us)
Async XLA Ops:
  6.5 2.4 %copy-start.2 = (bf16[1,128,2048]{2,1,0:T(8,128)(2,1)S(1)}, bf16[1,128,2048]{2,1,0:T(8,128)(2,1)}, u32[]{:S(2)}) copy-start(bf16[1,128,2048]{2,1,0:T(8,128)(2,1)} %param.5) | copy-start | bytes 1572868
  6.5 23.7 %all-gather.2.cloned.1.call-start = ((), (), s32[]{:S(2)}) async-start(), calls=%async_computation.2 | async-start | bytes 3145728 | tf_op jit(solution)/shard_map/all_gather | solution.py:49
  8.9 5.4 %copy-start.3 = (bf16[4,2048]{1,0:T(4,128)(2,1)S(1)}, bf16[4,2048]{1,0:T(4,128)(2,1)}, u32[]{:S(2)}) copy-start(bf16[4,2048]{1,0:T(4,128)(2,1)} %param.6) | copy-start | bytes 49156
  9.4 16.0 %collective-permute-start = (bf16[2048,3]{1,0:T(8,128)(2,1)S(1)}, bf16[2048,3]{1,0:T(8,128)(2,1)S(1)}, u32[]{:S(2)}, u32[]{:S(2)}) collective-permute-start(bf16[2048,3]{1,0:T(8,128)(2,1)S(1)} %slice.406), channel_id=1, source_target_pairs={{0,2},{2,4},{4,6},{6,8},{8,10},{10,12},{12,14},{14,16},{16,18},{18... | collective-permute-start | bytes 36872 | tf_op jit(solution)/shard_map/ppermute | solution.py:15
  43.5 8.8 %copy-start.4 = (f32[1,2048]{1,0:T(1,128)S(1)}, f32[1,2048]{1,0:T(1,128)}, u32[]{:S(2)}) copy-start(f32[1,2048]{1,0:T(1,128)} %param.9) | copy-start | bytes 24580
  43.5 41.5 %all-to-all-start = ((bf16[16,3,128,128]{3,2,1,0:T(8,128)(2,1)}), bf16[16,3,128,128]{3,2,1,0:T(8,128)(2,1)S(1)}, u32[]{:S(2)}, u32[]{:S(2)}) async-start(bf16[16,3,128,128]{3,2,1,0:T(8,128)(2,1)} %fusion.10), calls=%async_computation | async-start | bytes 3145728 | tf_op jit(solution)/shard_map/all_to_all | solution.py:57
  87.6 2.7 %copy-start = (f32[1,128,16,128]{3,1,0,2:T(8,128)S(1)}, f32[1,128,16,128]{3,1,0,2:T(8,128)}, u32[]{:S(2)}) copy-start(f32[1,128,16,128]{3,1,0,2:T(8,128)} %get-tuple-element.5) | copy-start | bytes 3145732
  99.0 4.8 %copy-start.1 = (f32[128,1024]{0,1:T(8,128)S(1)}, f32[128,1024]{0,1:T(8,128)}, u32[]{:S(2)}) copy-start(f32[128,1024]{0,1:T(8,128)} %slice.324) | copy-start | bytes 1572868
Sparse Core Ops, SparseCore 0:
  9.0 13.2 all-gather.1
